TPU v7x, 32 devices: a whole 2x2x4 slice. The times are simulated.
32 devices in a mesh: ep: 8 (over z, y), tp: 4 (over x, core).
Axes of the slice: x: 2, y: 2, z: 4, core: 2. Of those that a mesh axis runs over, the one named last changes fastest.
Arguments:
- mixer_input_rows: bfloat16 [4096, 2048], P(('ep', 'tp')), may hold values from -6 to 6
- mixer_norm_scale: float32 [2048], replicated, may hold values from 0.1 to 1.9
- decay_bias_table: float32 [4096, 16], P('ep', 'tp'), may hold values from -14 to 1
- erase_bias_table: float32 [16], P('tp'), may hold values from -12 to 1
- receive_weight: bfloat16 [2048, 1024], P(None, 'tp'), may hold values from -0.125 to 0.125
- key_weight: bfloat16 [2048, 1024], P(None, 'tp'), may hold values from -0.125 to 0.125
- value_weight: bfloat16 [2048, 1024], P(None, 'tp'), may hold values from -0.125 to 0.125
- decay_weight: bfloat16 [2048, 1024], P(None, 'tp'), may hold values from -0.125 to 0.125
- erase_weight: bfloat16 [2048, 1024], P(None, 'tp'), may hold values from -0.125 to 0.125
- self_token_scale: float32 [16, 64], P('tp'), may hold values from -0.6 to 0.6
- head_norm_scale: float32 [1024], P('tp'), may hold values from 0.1 to 1.9
- output_weight: bfloat16 [1024, 2048], P('tp'), may hold values from -0.1875 to 0.1875
- expert_input_rows: bfloat16 [4096, 2048], P(('ep', 'tp')), may hold values from -6 to 6
- expert_norm_scale: float32 [2048], replicated, may hold values from 0.1 to 1.9
- routes: int32 [4096, 2], P(('ep', 'tp')), may hold values from 0 to 31, all different within a row; in each aligned block of 128 rows (0 to 127, 128 to 255, ...) at most 16 rows name the same one
- router_weights: float32 [4096, 2], P(('ep', 'tp')), may hold values from 0.1 to 1
- routed_gate_weight: bfloat16 [32, 2048, 1024], P(('ep', 'tp')), may hold values from -0.125 to 0.125
- routed_up_weight: bfloat16 [32, 2048, 1024], P(('ep', 'tp')), may hold values from -0.125 to 0.125
- routed_down_weight: bfloat16 [32, 1024, 2048], P(('ep', 'tp')), may hold values from -0.1875 to 0.1875
- common_gate_weight: bfloat16 [2048, 256], replicated, may hold values from -0.125 to 0.125
- common_up_weight: bfloat16 [2048, 256], replicated, may hold values from -0.125 to 0.125
- common_down_weight: bfloat16 [256, 2048], replicated, may hold values from -0.375 to 0.375
Outputs:
- mixer_output: bfloat16 [4096, 2048], P(('ep', 'tp'))
- mixed_b: bfloat16 [4096, 2048], P(('ep', 'tp'))
Inputs may be any that keep to these rules, and one draw needn't show every extreme that they name: `routes`: within the rows of one device no expert is named by more than 16 rows, a bound that some block reaches; each row names 2 different experts, and every expert is named somewhere.
All inputs are finite; a program needn't handle non-finite values.
Results may differ from a plain program's by a relative error of at most 0.015.
Values may be sent and summed in bfloat16 or wider, within the bound.
A program may use at most 128 MiB of HBM per device.

v0:
```python
import jax
import jax.numpy as jnp
from jax import lax
from jax.sharding import PartitionSpec as P

precise = lax.Precision.HIGHEST


def passed_along(value, axis, by):
    peers = lax.axis_size(axis)
    pairs = [(i, i + by) for i in range(peers) if 0 <= i + by < peers]
    return lax.ppermute(value, axis, pairs)


def rms_rows(values, feature_gain):
    wide_values = values.astype(jnp.float32)
    inverse = lax.rsqrt(jnp.mean(wide_values * wide_values, axis=1, keepdims=True) + 1e-06)
    return (wide_values * inverse * feature_gain).astype(jnp.bfloat16)


def masked_pairs(left_rows, right_rows, keep_mask):
    products = jnp.einsum("htk,hsk->hts", left_rows, right_rows, precision=precise)
    return jnp.where(keep_mask[None], products, 0.0)


def block_pass(state_in, inputs):
    receive_vector, log_decay, key_projected, value_projected, unit_key, erase_rate = inputs
    block_len = receive_vector.shape[1]
    positions = jnp.arange(block_len)
    strict_mask = positions[:, None] > positions[None, :]
    causal_mask = positions[:, None] >= positions[None, :]
    cumulative = jnp.cumsum(log_decay, axis=1)
    growth = jnp.exp(-cumulative)
    erase_in = -unit_key * jnp.exp(cumulative - log_decay)
    erase_out = unit_key * erase_rate * growth
    key_out = key_projected * growth
    read_in = receive_vector * jnp.exp(cumulative)
    value_aug = jnp.concatenate([value_projected, jnp.zeros_like(value_projected)], axis=2)
    mix_erase = masked_pairs(erase_in, erase_out, strict_mask)
    mix_key = masked_pairs(erase_in, key_out, strict_mask)
    read_erase = masked_pairs(read_in, erase_out, causal_mask)
    read_key = masked_pairs(read_in, key_out, causal_mask)
    right_side = jnp.einsum("hvk,htk->htv", state_in, erase_in, precision=precise) + jnp.einsum(
        "hts,hsv->htv", mix_key, value_aug, precision=precise
    )
    system = jnp.eye(block_len, dtype=jnp.float32)[None] - mix_erase
    erased = jax.scipy.linalg.solve_triangular(system, right_side, lower=True, unit_diagonal=True)
    outputs = (
        jnp.einsum("hvk,htk->htv", state_in, read_in, precision=precise)
        + jnp.einsum("hts,hsv->htv", read_erase, erased, precision=precise)
        + jnp.einsum("hts,hsv->htv", read_key, value_aug, precision=precise)
    )
    decay_tail = jnp.exp(cumulative[:, -1:, :] - cumulative)
    state_out = (
        state_in * jnp.exp(cumulative[:, -1, :])[:, None, :]
        + jnp.einsum("htv,htk->hvk", erased, unit_key * erase_rate * decay_tail, precision=precise)
        + jnp.einsum("htv,htk->hvk", value_aug, key_projected * decay_tail, precision=precise)
    )
    return (state_out, outputs)


def local_states(receive_vector, log_decay, key_projected, value_projected, unit_key, erase_rate):
    row_count, head_count, head_channel_count = receive_vector.shape
    block_len = min(64, row_count)
    block_count = row_count // block_len

    def blocked(field_rows):
        return field_rows.reshape(block_count, block_len, head_count, head_channel_count).transpose(
            0, 2, 1, 3
        )

    identity_part = jnp.broadcast_to(
        jnp.eye(head_channel_count, dtype=jnp.float32),
        (head_count, head_channel_count, head_channel_count),
    )
    start_state = jnp.concatenate(
        [
            jnp.zeros((head_count, head_channel_count, head_channel_count), jnp.float32),
            identity_part,
        ],
        axis=1,
    )
    members = (receive_vector, log_decay, key_projected, value_projected, unit_key, erase_rate)
    final_state, outputs = lax.scan(
        block_pass, start_state, tuple((blocked(member) for member in members))
    )
    outputs = outputs.transpose(0, 2, 1, 3).reshape(row_count, head_count, 2 * head_channel_count)
    return (final_state, outputs)


def per_device(
    mixer_input_rows,
    mixer_norm_scale,
    decay_bias_table,
    erase_bias_table,
    receive_weight,
    key_weight,
    value_weight,
    decay_weight,
    erase_weight,
    self_token_scale,
    head_norm_scale,
    output_weight,
    expert_input_rows,
    expert_norm_scale,
    routes,
    router_weights,
    routed_gate_weight,
    routed_up_weight,
    routed_down_weight,
    common_gate_weight,
    common_up_weight,
    common_down_weight,
):
    normed_a = rms_rows(mixer_input_rows, mixer_norm_scale)
    local_width = key_weight.shape[1]
    row_piece = lax.all_gather(normed_a, "tp", axis=0, tiled=True)
    projected = jnp.concatenate(
        [
            jnp.dot(row_piece, weight_part, preferred_element_type=jnp.float32)
            for weight_part in (
                receive_weight,
                key_weight,
                value_weight,
                decay_weight,
                erase_weight,
            )
        ],
        axis=1,
    )
    row_count = projected.shape[0]
    head_channel_count = self_token_scale.shape[1]
    head_count = local_width // head_channel_count

    def head_slice(index_part):
        columns = projected[:, index_part * local_width : (index_part + 1) * local_width]
        return columns.reshape(row_count, head_count, head_channel_count)

    receive_vector = head_slice(0)
    key_projected = head_slice(1)
    value_projected = head_slice(2)
    log_decay = -jnp.exp(-jax.nn.softplus(-(head_slice(3) + decay_bias_table[:, :, None])) - 0.5)
    erase_rate = jax.nn.sigmoid(head_slice(4) + erase_bias_table[None, :, None])
    unit_key = key_projected * lax.rsqrt(
        jnp.sum(key_projected * key_projected, axis=2, keepdims=True) + 1e-06
    )
    final_state, outputs = local_states(
        receive_vector, log_decay, key_projected, value_projected, unit_key, erase_rate
    )
    state_local = final_state[:, :head_channel_count]
    transit = final_state[:, head_channel_count:]

    def relay_state(turn_index, entering_state):
        leaving = (
            jnp.einsum("hvj,hjk->hvk", entering_state, transit, precision=precise) + state_local
        )
        return passed_along(leaving.astype(jnp.bfloat16), "ep", 1).astype(leaving.dtype)

    entering = lax.fori_loop(0, lax.axis_size("ep") - 1, relay_state, jnp.zeros_like(state_local))
    readout = outputs[:, :, :head_channel_count] + jnp.einsum(
        "hvk,thk->thv", entering, outputs[:, :, head_channel_count:], precision=precise
    )
    mean_removed = readout - jnp.mean(readout, axis=2, keepdims=True)
    squared_mean = jnp.mean(mean_removed * mean_removed, axis=2, keepdims=True)
    head_norm_scales = head_norm_scale.reshape(head_count, head_channel_count)
    self_token_term = (
        jnp.sum(receive_vector * key_projected * self_token_scale[None], axis=2, keepdims=True)
        * value_projected
    )
    mixer_head_count = (
        mean_removed * lax.rsqrt(squared_mean + 0.00064) * head_norm_scales + self_token_term
    )
    mixer_head_count = mixer_head_count.reshape(row_count, local_width).astype(jnp.bfloat16)
    mixer_output = lax.psum_scatter(
        jnp.dot(mixer_head_count, output_weight, preferred_element_type=jnp.float32).astype(
            jnp.bfloat16
        ),
        "tp",
        scatter_dimension=0,
        tiled=True,
    )
    normed_b = rms_rows(expert_input_rows, expert_norm_scale)
    route_weight = 2.5 * router_weights / jnp.sum(router_weights, axis=1, keepdims=True)
    token_count, top_count = routes.shape
    expert_count = lax.axis_size("ep") * lax.axis_size("tp")
    capacity = 2 * token_count * top_count // expert_count
    chosen = routes.reshape(-1)
    onehot = (chosen[:, None] == jnp.arange(expert_count, dtype=jnp.int32)[None, :]).astype(
        jnp.int32
    )
    slot_rank = jnp.sum(jnp.cumsum(onehot, axis=0) * onehot, axis=1) - 1
    slot_index = chosen * capacity + slot_rank
    owners = jnp.arange(token_count * top_count, dtype=jnp.int32) // top_count
    source_row = jnp.zeros((expert_count * capacity,), jnp.int32).at[slot_index].set(owners)
    filled = jnp.zeros((expert_count * capacity,), jnp.bfloat16).at[slot_index].set(1.0)
    outgoing = (normed_b[source_row] * filled[:, None]).reshape(expert_count, capacity, -1)
    gate_part = routed_gate_weight[0]
    up_part = routed_up_weight[0]
    down_part = routed_down_weight[0]
    arrived = lax.all_to_all(outgoing, ("ep", "tp"), split_axis=0, concat_axis=0, tiled=True)
    flat_rows = arrived.reshape(-1, arrived.shape[-1])
    expert_hidden = (
        jax.nn.silu(jnp.dot(flat_rows, gate_part, preferred_element_type=jnp.float32))
        * jnp.dot(flat_rows, up_part, preferred_element_type=jnp.float32)
    ).astype(jnp.bfloat16)
    result = jnp.dot(expert_hidden, down_part, preferred_element_type=jnp.float32).astype(
        jnp.bfloat16
    )
    returned = lax.all_to_all(
        result.reshape(arrived.shape), ("ep", "tp"), split_axis=0, concat_axis=0, tiled=True
    )
    back_rows = returned.reshape(expert_count * capacity, -1)
    picked = back_rows[slot_index].reshape(token_count, top_count, -1)
    routed = jnp.sum(picked * route_weight[:, :, None], axis=1)
    shared_hidden = (
        jax.nn.silu(jnp.dot(normed_b, common_gate_weight, preferred_element_type=jnp.float32))
        * jnp.dot(normed_b, common_up_weight, preferred_element_type=jnp.float32)
    ).astype(jnp.bfloat16)
    shared_term = jnp.dot(shared_hidden, common_down_weight, preferred_element_type=jnp.float32)
    mixed_b = (routed + shared_term).astype(jnp.bfloat16)
    return (mixer_output, mixed_b)


def solution(mesh):
    in_specs = (
        P(("ep", "tp"), None),
        P(),
        P("ep", "tp"),
        P("tp"),
        P(None, "tp"),
        P(None, "tp"),
        P(None, "tp"),
        P(None, "tp"),
        P(None, "tp"),
        P("tp", None),
        P("tp"),
        P("tp", None),
        P(("ep", "tp"), None),
        P(),
        P(("ep", "tp"), None),
        P(("ep", "tp"), None),
        P(("ep", "tp"), None, None),
        P(("ep", "tp"), None, None),
        P(("ep", "tp"), None, None),
        P(),
        P(),
        P(),
    )
    out_specs = (P(("ep", "tp"), None), P(("ep", "tp"), None))
    return jax.shard_map(
        per_device, mesh=mesh, in_specs=in_specs, out_specs=out_specs, check_vma=False
    )
```

profile of v0, /device:TPU:0, one launch (start us, length us, event | category | flops | bytes accessed | tf_op | source)
XLA Modules:
  0.0 488.4 jit_solution(15592319105124685723)
XLA Ops:
  8.6 2.0 fusion.48
  13.7 2.2 scatter_custom_fusion.1
  16.4 3.3 gather_fusion
  19.7 3.2 broadcast_multiply_fusion
  23.0 7.6 %all-to-all-start = ((bf16[32,16,2048]{2,1,0:T(8,128)(2,1)}), bf16[32,16,2048]{2,1,0:T(8,128)(2,1)}, u32[]{:S(2)}, u32[]{:S(2)}) async-start(bf16[32,16,2048]{2,1,0:T(8,128)(2,1)} %broadcast_multiply_fusion), calls=%async_computation.1 | async-start | bytes 4194304 | tf_op jit(solution)/shard_map/all_to_all | solution.py:200
  30.9 6.8 %all-gather.2.cloned.1.call-done = bf16[512,2048]{1,0:T(8,128)(2,1)} async-done(((bf16[128,2048]{1,0:T(8,128)(2,1)}), bf16[512,2048]{1,0:T(8,128)(2,1)}) %all-gather.2.cloned.1.call-update) | async-done | bytes 2097168 | tf_op jit(solution)/shard_map/all_gather | solution.py:117
  37.6 2.3 fusion.88
  41.4 2.7 fusion.89
  45.6 2.4 bitcast_reduce_fusion
  51.6 2.6 fusion.90
  55.4 2.6 copy.47
  58.0 3.7 fusion.85
  61.7 2.3 reshape_reshape.11
  64.0 2.6 copy.48
  68.5 2.3 fusion.56
  70.7 265.7 %while.23 = (s32[]{:T(128)}, f32[4,128,64]{1,2,0:T(8,128)S(1)}, f32[8,4,64,128]{3,2,0,1:T(8,128)}, f32[8,4,64,64]{3,2,1,0:T(8,128)}, f32[8,4,64,64]{3,2,1,0:T(8,...) while((s32[]{:T(128)}, f32[4,128,64]{1,2,0:T(8,128)S(1)}, ...), condition=%wide.region_4.5_spmd, body=%wide.region_2.4_spmd.sunk | while | flops 253341760 | bytes 6410905 | solution.py:84
  77.0 21.0 %custom-call.11 = f32[4,1,64,64]{2,3,1,0:T(8,128)} custom-call(f32[4,1,64,64]{3,2,1,0:T(8,128)} %fusion.165), custom_call_target="InvertDiagBlocksLowerTriangular" | custom-call | tf_op jit(solution)/shard_map/while/body/eval_jaxpr/jit(_solve_triangular)/vmap()/triangular_solve | solution.py:47
  110.3 21.0 %custom-call.11 = f32[4,1,64,64]{2,3,1,0:T(8,128)} custom-call(f32[4,1,64,64]{3,2,1,0:T(8,128)} %fusion.165), custom_call_target="InvertDiagBlocksLowerTriangular" | custom-call | tf_op jit(solution)/shard_map/while/body/eval_jaxpr/jit(_solve_triangular)/vmap()/triangular_solve | solution.py:47
  143.5 21.0 %custom-call.11 = f32[4,1,64,64]{2,3,1,0:T(8,128)} custom-call(f32[4,1,64,64]{3,2,1,0:T(8,128)} %fusion.165), custom_call_target="InvertDiagBlocksLowerTriangular" | custom-call | tf_op jit(solution)/shard_map/while/body/eval_jaxpr/jit(_solve_triangular)/vmap()/triangular_solve | solution.py:47
  176.7 21.0 %custom-call.11 = f32[4,1,64,64]{2,3,1,0:T(8,128)} custom-call(f32[4,1,64,64]{3,2,1,0:T(8,128)} %fusion.165), custom_call_target="InvertDiagBlocksLowerTriangular" | custom-call | tf_op jit(solution)/shard_map/while/body/eval_jaxpr/jit(_solve_triangular)/vmap()/triangular_solve | solution.py:47
  209.9 21.0 %custom-call.11 = f32[4,1,64,64]{2,3,1,0:T(8,128)} custom-call(f32[4,1,64,64]{3,2,1,0:T(8,128)} %fusion.165), custom_call_target="InvertDiagBlocksLowerTriangular" | custom-call | tf_op jit(solution)/shard_map/while/body/eval_jaxpr/jit(_solve_triangular)/vmap()/triangular_solve | solution.py:47
  243.1 21.0 %custom-call.11 = f32[4,1,64,64]{2,3,1,0:T(8,128)} custom-call(f32[4,1,64,64]{3,2,1,0:T(8,128)} %fusion.165), custom_call_target="InvertDiagBlocksLowerTriangular" | custom-call | tf_op jit(solution)/shard_map/while/body/eval_jaxpr/jit(_solve_triangular)/vmap()/triangular_solve | solution.py:47
  276.3 21.0 %custom-call.11 = f32[4,1,64,64]{2,3,1,0:T(8,128)} custom-call(f32[4,1,64,64]{3,2,1,0:T(8,128)} %fusion.165), custom_call_target="InvertDiagBlocksLowerTriangular" | custom-call | tf_op jit(solution)/shard_map/while/body/eval_jaxpr/jit(_solve_triangular)/vmap()/triangular_solve | solution.py:47
  309.5 21.0 %custom-call.11 = f32[4,1,64,64]{2,3,1,0:T(8,128)} custom-call(f32[4,1,64,64]{3,2,1,0:T(8,128)} %fusion.165), custom_call_target="InvertDiagBlocksLowerTriangular" | custom-call | tf_op jit(solution)/shard_map/while/body/eval_jaxpr/jit(_solve_triangular)/vmap()/triangular_solve | solution.py:47
  336.4 2.3 copy.64
  338.9 49.8 %while.24 = (s32[]{:T(128)}, f32[4,64,64]{2,1,0:T(8,128)S(1)}, f32[4,64,64]{2,1,0:T(8,128)S(1)}, f32[4,64,64]{2,1,0:T(8,128)S(1)}, s32[]{:T(128)}, /*index=5*/s32[]{:T(128)}) while((s32[]{:T(128)}, f32[4,64,64]{2,1,0:T(8,128)S(1)}, f32[4,64,64]{2,1,0:T(8,128)S(1)}, f32[4,64,64]{2,1,0:T(8,128)S(1)}, s32[]{:T(128)}, ...), condition=%wide.region_6.7_spmd.clone, body=%wide.region_5.6_spmd.clone.sunk | while | flops 12648451 | bytes 458871 | solution.py:159
  339.4 3.6 collective-permute-start
  345.2 4.5 collective-permute-start
  349.8 1.9 collective-permute-done
  352.0 5.2 %collective-permute-start = (bf16[4,64,64]{2,1,0:T(8,128)(2,1)S(1)}, bf16[4,64,64]{2,1,0:T(8,128)(2,1)S(1)}, u32[]{:S(2)}, u32[]{:S(2)}) collective-permute-start(bf16[4,64,64]{2,1,0:T(8,128)(2,1)S(1)} %fusion.171), channel_id=1, source_target_pairs={{0,4},{4,8},{8,12},{12,16},{16,20},{20,24},{24,28},{1,5},{5,9},{9,... | collective-permute-start | bytes 98312 | tf_op jit(solution)/shard_map/while/body/eval_jaxpr/ppermute | solution.py:12
  357.1 1.9 collective-permute-done
  359.3 5.2 %collective-permute-start = (bf16[4,64,64]{2,1,0:T(8,128)(2,1)S(1)}, bf16[4,64,64]{2,1,0:T(8,128)(2,1)S(1)}, u32[]{:S(2)}, u32[]{:S(2)}) collective-permute-start(bf16[4,64,64]{2,1,0:T(8,128)(2,1)S(1)} %fusion.171), channel_id=1, source_target_pairs={{0,4},{4,8},{8,12},{12,16},{16,20},{20,24},{24,28},{1,5},{5,9},{9,... | collective-permute-start | bytes 98312 | tf_op jit(solution)/shard_map/while/body/eval_jaxpr/ppermute | solution.py:12
  364.5 1.9 collective-permute-done
  366.7 5.2 %collective-permute-start = (bf16[4,64,64]{2,1,0:T(8,128)(2,1)S(1)}, bf16[4,64,64]{2,1,0:T(8,128)(2,1)S(1)}, u32[]{:S(2)}, u32[]{:S(2)}) collective-permute-start(bf16[4,64,64]{2,1,0:T(8,128)(2,1)S(1)} %fusion.171), channel_id=1, source_target_pairs={{0,4},{4,8},{8,12},{12,16},{16,20},{20,24},{24,28},{1,5},{5,9},{9,... | collective-permute-start | bytes 98312 | tf_op jit(solution)/shard_map/while/body/eval_jaxpr/ppermute | solution.py:12
  371.9 1.9 collective-permute-done
  374.0 5.2 %collective-permute-start = (bf16[4,64,64]{2,1,0:T(8,128)(2,1)S(1)}, bf16[4,64,64]{2,1,0:T(8,128)(2,1)S(1)}, u32[]{:S(2)}, u32[]{:S(2)}) collective-permute-start(bf16[4,64,64]{2,1,0:T(8,128)(2,1)S(1)} %fusion.171), channel_id=1, source_target_pairs={{0,4},{4,8},{8,12},{12,16},{16,20},{20,24},{24,28},{1,5},{5,9},{9,... | collective-permute-start | bytes 98312 | tf_op jit(solution)/shard_map/while/body/eval_jaxpr/ppermute | solution.py:12
  379.2 2.5 collective-permute-done
  382.0 4.9 %collective-permute-start = (bf16[4,64,64]{2,1,0:T(8,128)(2,1)S(1)}, bf16[4,64,64]{2,1,0:T(8,128)(2,1)S(1)}, u32[]{:S(2)}, u32[]{:S(2)}) collective-permute-start(bf16[4,64,64]{2,1,0:T(8,128)(2,1)S(1)} %fusion.171), channel_id=1, source_target_pairs={{0,4},{4,8},{8,12},{12,16},{16,20},{20,24},{24,28},{1,5},{5,9},{9,... | collective-permute-start | bytes 98312 | tf_op jit(solution)/shard_map/while/body/eval_jaxpr/ppermute | solution.py:12
  388.8 2.5 fusion.86
  391.4 6.5 %fusion.33 = f32[512,1024]{1,0:T(8,128)} fusion(bf16[512,2048]{1,0:T(8,128)(2,1)} %bitcast.29, bf16[1,2048,1024]{2,1,0:T(8,128)(2,1)} %param.42), kind=kOutput, calls=%fused_computation.65 | convolution fusion | flops 2147483648 | bytes 8388608 | tf_op jit(solution)/shard_map/dot_general | solution.py:203
  397.9 10.5 %fusion.35 = bf16[512,2048]{1,0:T(8,128)(2,1)} fusion(bf16[1,1024,2048]{2,1,0:T(8,128)(2,1)} %param.44, f32[512,1024]{1,0:T(8,128)} %fusion.33, bf16[512,2048]{1,0:T(8,128)(2,1)} %bitcast.29, bf16[1,2048,1024]{2,1,0:T(8,128)(2,1)} %param.43), kind=kOutput, calls=%fused_computation.68 | convolution fusion | flops 4299161600 | bytes 14680064 | tf_op jit(solution)/shard_map/dot_general | solution.py:206
  408.4 9.7 %all-to-all-start.1 = ((bf16[32,16,2048]{2,1,0:T(8,128)(2,1)}), bf16[32,16,2048]{2,1,0:T(8,128)(2,1)}, u32[]{:S(2)}, u32[]{:S(2)}) async-start(bf16[32,16,2048]{2,1,0:T(8,128)(2,1)} %bitcast.205), calls=%async_computation.2 | async-start | bytes 4194304 | tf_op jit(solution)/shard_map/all_to_all | solution.py:209
  418.4 2.1 convolution_convert_fusion
  422.1 44.8 %all-to-all-done.1 = bf16[32,16,2048]{2,1,0:T(8,128)(2,1)} async-done(((bf16[32,16,2048]{2,1,0:T(8,128)(2,1)}), bf16[32,16,2048]{2,1,0:T(8,128)(2,1)}, u32[]{:S(2)}, u32[]{:S(2)}) %all-to-all-start.1) | async-done | bytes 2097184 | tf_op jit(solution)/shard_map/all_to_all | solution.py:209
  466.9 4.2 gather_fusion.1
  471.1 2.6 reshape.198
  473.7 4.7 multiply_reduce_fusion
  478.5 3.1 fusion.38
  (281 shorter events, 119.3 us)
Async XLA Ops:
  7.2 411.3 %copy-start = (bf16[256,2048]{1,0:T(8,128)(2,1)S(1)}, bf16[256,2048]{1,0:T(8,128)(2,1)}, u32[]{:S(2)}) copy-start(bf16[256,2048]{1,0:T(8,128)(2,1)} %param.37) | copy-start | bytes 3145732
  7.2 3.5 copy-start.12
  7.2 8.8 %copy-start.8 = (bf16[128,2048]{1,0:T(8,128)(2,1)S(1)}, bf16[128,2048]{1,0:T(8,128)(2,1)}, u32[]{:S(2)}) copy-start(bf16[128,2048]{1,0:T(8,128)(2,1)} %param.38) | copy-start | bytes 1572868
  7.2 9.0 %copy-start.10 = (f32[2048]{0:T(1024)S(1)}, f32[2048]{0:T(1024)}, u32[]{:S(2)}) copy-start(f32[2048]{0:T(1024)} %param.39) | copy-start | bytes 24580
  7.2 30.4 %all-gather.2.cloned.1.call-start = ((), (), s32[]{:S(2)}) async-start(), calls=%async_computation.3 | async-start | bytes 2621440 | tf_op jit(solution)/shard_map/all_gather | solution.py:117
  23.0 7.6 %copy-start.11 = (f32[512,4]{0,1:T(4,128)S(1)}, f32[512,4]{0,1:T(4,128)}, u32[]{:S(2)}) copy-start(f32[512,4]{0,1:T(4,128)} %param.28) | copy-start | bytes 24580
  23.0 7.7 %copy-start.15 = (f32[256]{0:T(256)S(1)}, f32[256]{0:T(256)}, u32[]{:S(2)}) copy-start(f32[256]{0:T(256)} %param.36) | copy-start | bytes 3076
  23.0 14.7 %copy-start.17 = (bf16[2048,256]{1,0:T(8,128)(2,1)S(1)}, bf16[2048,256]{1,0:T(8,128)(2,1)}, u32[]{:S(2)}) copy-start(bf16[2048,256]{1,0:T(8,128)(2,1)} %param.33) | copy-start | bytes 3145732
  23.0 368.4 %all-to-all-start = ((bf16[32,16,2048]{2,1,0:T(8,128)(2,1)}), bf16[32,16,2048]{2,1,0:T(8,128)(2,1)}, u32[]{:S(2)}, u32[]{:S(2)}) async-start(bf16[32,16,2048]{2,1,0:T(8,128)(2,1)} %broadcast_multiply_fusion), calls=%async_computation.1 | async-start | bytes 4194304 | tf_op jit(solution)/shard_map/all_to_all | solution.py:200
  41.4 4.2 copy-start.18
  47.9 0.8 copy-start.7
  54.2 7.5 %copy-start.4 = (f32[512,256]{0,1:T(8,128)}, f32[512,256]{0,1:T(8,128)S(1)}, u32[]{:S(2)}) copy-start(f32[512,256]{0,1:T(8,128)S(1)} %fusion.90) | copy-start | bytes 1572868
  64.0 3.9 copy-start.16
  66.5 1.4 copy-start.1
  66.5 1.9 copy-start.2
  338.7 50.0 %copy-start.3 = (f32[8,4,64,128]{3,2,0,1:T(8,128)S(1)}, f32[8,4,64,128]{3,2,0,1:T(8,128)}, u32[]{:S(2)}) copy-start(f32[8,4,64,128]{3,2,0,1:T(8,128)} %get-tuple-element.72) | copy-start | bytes 3145732
  339.4 5.5 %collective-permute-start = (bf16[4,64,64]{2,1,0:T(8,128)(2,1)S(1)}, bf16[4,64,64]{2,1,0:T(8,128)(2,1)S(1)}, u32[]{:S(2)}, u32[]{:S(2)}) collective-permute-start(bf16[4,64,64]{2,1,0:T(8,128)(2,1)S(1)} %fusion.171), channel_id=1, source_target_pairs={{0,4},{4,8},{8,12},{12,16},{16,20},{20,24},{24,28},{1,5},{5,9},{9,... | collective-permute-start | bytes 98312 | tf_op jit(solution)/shard_map/while/body/eval_jaxpr/ppermute | solution.py:12
  345.2 6.4 %collective-permute-start = (bf16[4,64,64]{2,1,0:T(8,128)(2,1)S(1)}, bf16[4,64,64]{2,1,0:T(8,128)(2,1)S(1)}, u32[]{:S(2)}, u32[]{:S(2)}) collective-permute-start(bf16[4,64,64]{2,1,0:T(8,128)(2,1)S(1)} %fusion.171), channel_id=1, source_target_pairs={{0,4},{4,8},{8,12},{12,16},{16,20},{20,24},{24,28},{1,5},{5,9},{9,... | collective-permute-start | bytes 98312 | tf_op jit(solution)/shard_map/while/body/eval_jaxpr/ppermute | solution.py:12
  352.0 7.1 %collective-permute-start = (bf16[4,64,64]{2,1,0:T(8,128)(2,1)S(1)}, bf16[4,64,64]{2,1,0:T(8,128)(2,1)S(1)}, u32[]{:S(2)}, u32[]{:S(2)}) collective-permute-start(bf16[4,64,64]{2,1,0:T(8,128)(2,1)S(1)} %fusion.171), channel_id=1, source_target_pairs={{0,4},{4,8},{8,12},{12,16},{16,20},{20,24},{24,28},{1,5},{5,9},{9,... | collective-permute-start | bytes 98312 | tf_op jit(solution)/shard_map/while/body/eval_jaxpr/ppermute | solution.py:12
  359.3 7.1 %collective-permute-start = (bf16[4,64,64]{2,1,0:T(8,128)(2,1)S(1)}, bf16[4,64,64]{2,1,0:T(8,128)(2,1)S(1)}, u32[]{:S(2)}, u32[]{:S(2)}) collective-permute-start(bf16[4,64,64]{2,1,0:T(8,128)(2,1)S(1)} %fusion.171), channel_id=1, source_target_pairs={{0,4},{4,8},{8,12},{12,16},{16,20},{20,24},{24,28},{1,5},{5,9},{9,... | collective-permute-start | bytes 98312 | tf_op jit(solution)/shard_map/while/body/eval_jaxpr/ppermute | solution.py:12
  366.7 7.1 %collective-permute-start = (bf16[4,64,64]{2,1,0:T(8,128)(2,1)S(1)}, bf16[4,64,64]{2,1,0:T(8,128)(2,1)S(1)}, u32[]{:S(2)}, u32[]{:S(2)}) collective-permute-start(bf16[4,64,64]{2,1,0:T(8,128)(2,1)S(1)} %fusion.171), channel_id=1, source_target_pairs={{0,4},{4,8},{8,12},{12,16},{16,20},{20,24},{24,28},{1,5},{5,9},{9,... | collective-permute-start | bytes 98312 | tf_op jit(solution)/shard_map/while/body/eval_jaxpr/ppermute | solution.py:12
  374.0 7.6 %collective-permute-start = (bf16[4,64,64]{2,1,0:T(8,128)(2,1)S(1)}, bf16[4,64,64]{2,1,0:T(8,128)(2,1)S(1)}, u32[]{:S(2)}, u32[]{:S(2)}) collective-permute-start(bf16[4,64,64]{2,1,0:T(8,128)(2,1)S(1)} %fusion.171), channel_id=1, source_target_pairs={{0,4},{4,8},{8,12},{12,16},{16,20},{20,24},{24,28},{1,5},{5,9},{9,... | collective-permute-start | bytes 98312 | tf_op jit(solution)/shard_map/while/body/eval_jaxpr/ppermute | solution.py:12
  382.0 6.8 %collective-permute-start = (bf16[4,64,64]{2,1,0:T(8,128)(2,1)S(1)}, bf16[4,64,64]{2,1,0:T(8,128)(2,1)S(1)}, u32[]{:S(2)}, u32[]{:S(2)}) collective-permute-start(bf16[4,64,64]{2,1,0:T(8,128)(2,1)S(1)} %fusion.171), channel_id=1, source_target_pairs={{0,4},{4,8},{8,12},{12,16},{16,20},{20,24},{24,28},{1,5},{5,9},{9,... | collective-permute-start | bytes 98312 | tf_op jit(solution)/shard_map/while/body/eval_jaxpr/ppermute | solution.py:12
  408.4 9.8 %copy-start.5 = (f32[512,256]{0,1:T(8,128)S(1)}, f32[512,256]{0,1:T(8,128)}, u32[]{:S(2)}) copy-start(f32[512,256]{0,1:T(8,128)} %copy-done.4) | copy-start | bytes 1572868
  408.4 9.8 %copy-start.6 = (f32[512,256]{0,1:T(8,128)S(1)}, f32[512,256]{0,1:T(8,128)}, u32[]{:S(2)}) copy-start(f32[512,256]{0,1:T(8,128)} %get-tuple-element.126) | copy-start | bytes 1572868
  408.4 9.8 %copy-start.14 = (f32[4,64]{1,0:T(4,128)S(1)}, f32[4,64]{1,0:T(4,128)}, u32[]{:S(2)}) copy-start(f32[4,64]{1,0:T(4,128)} %param.35) | copy-start | bytes 3076
  408.4 58.5 %all-to-all-start.1 = ((bf16[32,16,2048]{2,1,0:T(8,128)(2,1)}), bf16[32,16,2048]{2,1,0:T(8,128)(2,1)}, u32[]{:S(2)}, u32[]{:S(2)}) async-start(bf16[32,16,2048]{2,1,0:T(8,128)(2,1)} %bitcast.205), calls=%async_computation.2 | async-start | bytes 4194304 | tf_op jit(solution)/shard_map/all_to_all | solution.py:209
  418.1 63.5 %reduce-scatter.2.cloned.1.call-start = ((), (), s32[]{:S(2)}) async-start(), calls=%async_computation.4 | async-start | bytes 2621440 | tf_op jit(solution)/shard_map/reduce_scatter | solution.py:174
  420.5 0.7 copy-start.13
  420.5 1.2 copy-start.9
Sparse Core Ops, SparseCore 0:
  10.8 26.8 all-gather.1
  422.0 36.8 reduce-scatter.1
where the time goes:
time: 491 us; the launch traced here: 488 us
  other arithmetic  203 us (41%)
  matrix products  111 us (23%)
  waiting for transfers between devices  65.4 us (13%)
  starting transfers between devices  51.1 us (10%)
  local copies, waits for them, and re-layouts  42.3 us (9%)
  between operations  14.4 us (3%)
    another operation x16, other arithmetic, block_pass(): jax.scipy.linalg.solve_triangular(system, right_side, lower=True, unit_di...  168 us
    all_to_all x1, waiting for transfers between devices, per_device(): lax.all_to_all(result.reshape(arrived.shape), ('ep', 'tp'), split_axis=0,...  44.8 us
    ppermute x7, starting transfers between devices, passed_along(): return lax.ppermute(value, axis, pairs)  33.7 us
    dot_general x32, matrix products, masked_pairs(): jnp.einsum('htk,hsk->hts', left_rows, right_rows, precision=precise)  31.2 us
    ppermute x7, waiting for transfers between devices, passed_along(): return lax.ppermute(value, axis, pairs)  13.8 us
    dot_general x5, matrix products, per_device(): jnp.dot(row_piece, weight_part, preferred_element_type=jnp.float32)  13.6 us
    another operation x6, local copies, waits for them, and re-layouts, blocked(): field_rows.reshape(block_count, block_len, head_count, head_channel_count)  11.4 us
    dot_general x1, matrix products, per_device(): jnp.dot(expert_hidden, down_part, preferred_element_type=jnp.float32)  10.5 us
  transfers between devices with their start and end apart: 11, of which 9 were waited for; matrix products, arithmetic and copies ran while one was open for 68% of the time, Pallas kernels for 0%

commit v1 on v0

v1 whole, which is shorter than its diff:
```python
import functools

import jax
import jax.numpy as jnp
from jax import lax
from jax.experimental import pallas as pl
from jax.experimental.pallas import tpu as pltpu
from jax.sharding import PartitionSpec as P

precise = lax.Precision.HIGHEST


def rms_rows(values, feature_gain):
    wide_values = values.astype(jnp.float32)
    inverse = lax.rsqrt(jnp.mean(wide_values * wide_values, axis=1, keepdims=True) + 1e-06)
    return (wide_values * inverse * feature_gain).astype(jnp.bfloat16)


def halves(wide):
    high = wide.astype(jnp.bfloat16)
    return high, (wide - high.astype(jnp.float32)).astype(jnp.bfloat16)


def split_dot(left, right, left_axis, right_axis):
    left_high, left_low = halves(left)
    right_high, right_low = halves(right)
    return lax.dot_general(
        jnp.concatenate([left_high, left_high, left_low], axis=left_axis),
        jnp.concatenate([right_high, right_low, right_high], axis=right_axis),
        (((left_axis,), (right_axis,)), ((), ())),
        preferred_element_type=jnp.float32,
    )


def head_sums(wide, channels):
    rows, width = wide.shape
    same_head = (
        lax.broadcasted_iota(jnp.int32, (width, width), 0) // channels
        == lax.broadcasted_iota(jnp.int32, (width, width), 1) // channels
    )
    ones = jnp.where(same_head, 1.0, 0.0).astype(jnp.bfloat16)
    high, low = halves(wide)
    both = jnp.dot(
        jnp.concatenate([high, low], axis=0), ones, preferred_element_type=jnp.float32
    )
    return both[:rows] + both[rows:]


def scan_kernel(
    channels, block_len, r_ref, k_ref, v_ref, ld_ref, rate_ref, local_ref, through_ref, state_ref, aug_ref
):
    step = pl.program_id(0)
    width = r_ref.shape[1]
    heads = width // channels
    groups = r_ref.shape[0] // block_len

    def iotas(shape):
        return (
            lax.broadcasted_iota(jnp.int32, shape, 0),
            lax.broadcasted_iota(jnp.int32, shape, 1),
        )

    row, col = iotas((block_len, block_len))
    eye = jnp.where(row == col, 1.0, 0.0)
    wide_row, wide_col = iotas((2 * block_len, 2 * block_len))
    local_row, local_col = wide_row % block_len, wide_col % block_len
    keep = (local_row > local_col) | ((local_row == local_col) & (wide_row >= block_len))
    tri_row, tri_col = iotas((block_len, 3 * block_len))
    running = jnp.where(tri_row >= tri_col % block_len, 1.0, 0.0).astype(jnp.bfloat16)

    @pl.when(step == 0)
    def _():
        aug_row, aug_col = iotas((2 * channels, width))
        aug_ref[...] = jnp.where(aug_row - channels == aug_col % channels, 1.0, 0.0)

    pieces = []
    for group in range(groups):
        rows = pl.ds(group * block_len, block_len)
        receive, key, value = r_ref[rows, :], k_ref[rows, :], v_ref[rows, :]
        log_decay, rate = ld_ref[rows, :], rate_ref[rows, :]
        unit = key * lax.rsqrt(head_sums(key * key, channels) + 1e-06)
        high, rest = halves(log_decay)
        middle, low = halves(log_decay - high.astype(jnp.float32))
        cumulative = jnp.dot(
            running,
            jnp.concatenate([high, middle, low], axis=0),
            preferred_element_type=jnp.float32,
        )
        growth = jnp.exp(-cumulative)
        erase_in = -unit * jnp.exp(cumulative - log_decay)
        erase_out = unit * rate * growth
        key_out = key * growth
        read_in = receive * jnp.exp(cumulative)
        last = cumulative[block_len - 1 : block_len, :]
        tail = jnp.exp(last - cumulative)
        erase_tail = unit * rate * tail
        key_tail = key * tail
        total = jnp.exp(last)
        for head in range(heads):
            cut = slice(head * channels, (head + 1) * channels)
            products = split_dot(
                jnp.concatenate([erase_in[:, cut], read_in[:, cut]], axis=0),
                jnp.concatenate([erase_out[:, cut], key_out[:, cut]], axis=0),
                1,
                1,
            )
            products = jnp.where(keep, products, 0.0)
            pieces.append(
                dict(
                    group=group,
                    cut=cut,
                    products=products,
                    erase_in=erase_in[:, cut],
                    read_in=read_in[:, cut],
                    value=value[:, cut],
                    erase_tail=erase_tail[:, cut],
                    key_tail=key_tail[:, cut],
                    total=total[:, cut],
                    erase=products[:block_len, :block_len],
                )
            )
    for piece in pieces:
        piece["inverse"] = eye + jnp.where(row // 2 == col // 2, piece["erase"], 0.0)
    span = 2
    while span < block_len:
        joint = (row // (2 * span) == col // (2 * span)) & (row // span != col // span)
        for piece in pieces:
            piece["half"] = split_dot(piece["inverse"], jnp.where(joint, piece["erase"], 0.0), 1, 0)
        for piece in pieces:
            piece["inverse"] = piece["inverse"] + split_dot(piece["half"], piece["inverse"], 1, 0)
        span *= 2
    for piece in pieces:
        piece["valued"] = split_dot(piece["products"][:, block_len:], piece["value"], 1, 0)
    for piece in pieces:
        right = jnp.concatenate([piece["erase_in"], piece["valued"][:block_len]], axis=1)
        piece["erased"] = split_dot(piece["inverse"], right, 1, 0)
    for piece in pieces:
        read = split_dot(piece["products"][block_len:, :block_len], piece["erased"], 1, 0)
        piece["read_through"] = piece["read_in"] + read[:, :channels]
        piece["read_local"] = read[:, channels:] + piece["valued"][block_len:]
        piece["moved"] = split_dot(piece["erased"], piece["erase_tail"], 0, 0)
        piece["added"] = piece["moved"][channels:] + split_dot(
            piece["value"], piece["key_tail"], 0, 0
        )
    for piece in pieces:
        rows, cut = pl.ds(piece["group"] * block_len, block_len), piece["cut"]
        aug = aug_ref[:, cut]
        out = split_dot(piece["read_through"], aug, 1, 1)
        local_ref[rows, cut] = out[:, :channels] + piece["read_local"]
        through_ref[rows, cut] = out[:, channels:]
        after = aug * piece["total"] + split_dot(aug, piece["moved"][:channels], 1, 0)
        aug_ref[:, cut] = after + jnp.concatenate(
            [piece["added"], jnp.zeros_like(piece["added"])], axis=0
        )

    @pl.when(step == pl.num_programs(0) - 1)
    def _():
        state_ref[...] = aug_ref[...]


def local_scan(fields, channels):
    rows, width = fields[0].shape
    block_len = min(64, rows)
    tile = 2 * block_len if rows % (2 * block_len) == 0 else block_len
    tiled = pl.BlockSpec((tile, width), lambda i: (i, 0))
    return pl.pallas_call(
        functools.partial(scan_kernel, channels, block_len),
        grid=(rows // tile,),
        in_specs=[tiled] * 5,
        out_specs=[tiled, tiled, pl.BlockSpec((2 * channels, width), lambda i: (0, 0))],
        out_shape=[
            jax.ShapeDtypeStruct((rows, width), jnp.float32),
            jax.ShapeDtypeStruct((rows, width), jnp.float32),
            jax.ShapeDtypeStruct((2 * channels, width), jnp.float32),
        ],
        scratch_shapes=[pltpu.VMEM((2 * channels, width), jnp.float32)],
        compiler_params=pltpu.CompilerParams(dimension_semantics=("arbitrary",)),
        cost_estimate=pl.CostEstimate(
            flops=16 * 10**9, bytes_accessed=4 * 10**6, transcendentals=0
        ),
    )(*fields)


def read_kernel(
    channels,
    place_ref,
    states_ref,
    local_ref,
    through_ref,
    r_ref,
    k_ref,
    v_ref,
    own_ref,
    gain_ref,
    weight_ref,
    out_ref,
    enter_ref,
):
    width = local_ref.shape[1]
    cuts = [slice(at, at + channels) for at in range(0, width, channels)]

    @pl.when(pl.program_id(0) == 0)
    def _():
        enter_ref[...] = jnp.zeros_like(enter_ref)

        def one(index, carry):
            for cut in cuts:
                moved = jnp.dot(
                    enter_ref[:, cut],
                    states_ref[index, channels:, cut],
                    precision=precise,
                    preferred_element_type=jnp.float32,
                )
                enter_ref[:, cut] = moved + states_ref[index, :channels, cut]
            return carry

        lax.fori_loop(0, place_ref[0], one, 0)

    through = through_ref[...]
    readout = local_ref[...] + jnp.concatenate(
        [split_dot(through[:, cut], enter_ref[:, cut], 1, 1) for cut in cuts], axis=1
    )
    removed = readout - head_sums(readout, channels) * (1.0 / channels)
    squared = head_sums(removed * removed, channels) * (1.0 / channels)
    own = head_sums(r_ref[...] * k_ref[...] * own_ref[...], channels) * v_ref[...]
    mixed = removed * lax.rsqrt(squared + 0.00064) * gain_ref[...] + own
    out_ref[...] = jnp.dot(
        mixed.astype(jnp.bfloat16), weight_ref[...], preferred_element_type=jnp.float32
    ).astype(jnp.bfloat16)


def read_heads(place, states, local, through, receive, key, value, own, gain, weight, channels):
    rows, width = local.shape
    tile = min(128, rows)
    tiled = pl.BlockSpec((tile, width), lambda i: (i, 0))
    row_of = pl.BlockSpec((1, width), lambda i: (0, 0))
    return pl.pallas_call(
        functools.partial(read_kernel, channels),
        grid=(rows // tile,),
        in_specs=[
            pl.BlockSpec(memory_space=pltpu.SMEM),
            pl.BlockSpec(states.shape, lambda i: (0, 0, 0)),
            tiled,
            tiled,
            tiled,
            tiled,
            tiled,
            row_of,
            row_of,
            pl.BlockSpec(weight.shape, lambda i: (0, 0)),
        ],
        out_specs=pl.BlockSpec((tile, weight.shape[1]), lambda i: (i, 0)),
        out_shape=jax.ShapeDtypeStruct((rows, weight.shape[1]), jnp.bfloat16),
        scratch_shapes=[pltpu.VMEM((channels, width), jnp.float32)],
        compiler_params=pltpu.CompilerParams(dimension_semantics=("arbitrary",)),
        cost_estimate=pl.CostEstimate(
            flops=4 * 10**9, bytes_accessed=8 * 10**6, transcendentals=0
        ),
    )(place, states, local, through, receive, key, value, own, gain, weight)


def per_device(
    mixer_input_rows,
    mixer_norm_scale,
    decay_bias_table,
    erase_bias_table,
    receive_weight,
    key_weight,
    value_weight,
    decay_weight,
    erase_weight,
    self_token_scale,
    head_norm_scale,
    output_weight,
    expert_input_rows,
    expert_norm_scale,
    routes,
    router_weights,
    routed_gate_weight,
    routed_up_weight,
    routed_down_weight,
    common_gate_weight,
    common_up_weight,
    common_down_weight,
):
    normed_b = rms_rows(expert_input_rows, expert_norm_scale)
    route_weight = 2.5 * router_weights / jnp.sum(router_weights, axis=1, keepdims=True)
    token_count, top_count = routes.shape
    expert_count = lax.axis_size("ep") * lax.axis_size("tp")
    capacity = 2 * token_count * top_count // expert_count
    named = [
        routes[:, j : j + 1] == jnp.arange(expert_count, dtype=jnp.int32)[None, :]
        for j in range(top_count)
    ]
    counted = sum(n.astype(jnp.bfloat16) for n in named)
    token = jnp.arange(token_count)
    earlier = (token[:, None] > token[None, :]).astype(jnp.bfloat16)
    ranks = jnp.dot(earlier, counted, preferred_element_type=jnp.float32)
    slots = [
        routes[:, j] * capacity
        + jnp.sum(jnp.where(named[j], ranks, 0.0), axis=1).astype(jnp.int32)
        for j in range(top_count)
    ]
    slot_range = jnp.arange(expert_count * capacity, dtype=jnp.int32)
    chosen_rows = sum((slot_range[:, None] == s[None, :]).astype(jnp.bfloat16) for s in slots)
    outgoing = jnp.dot(chosen_rows, normed_b, preferred_element_type=jnp.float32)
    outgoing = outgoing.astype(jnp.bfloat16).reshape(expert_count, capacity, -1)
    arrived = lax.all_to_all(outgoing, ("ep", "tp"), split_axis=0, concat_axis=0, tiled=True)

    normed_a = rms_rows(mixer_input_rows, mixer_norm_scale)
    row_piece = lax.all_gather(normed_a, "tp", axis=0, tiled=True)
    channels = self_token_scale.shape[1]

    def projected(weight):
        return jnp.dot(row_piece, weight, preferred_element_type=jnp.float32)

    receive = projected(receive_weight)
    key = projected(key_weight)
    value = projected(value_weight)
    decay_in = projected(decay_weight) + jnp.repeat(decay_bias_table, channels, axis=1)
    log_decay = -jnp.exp(-jax.nn.softplus(-decay_in) - 0.5)
    rate = jax.nn.sigmoid(
        projected(erase_weight) + jnp.repeat(erase_bias_table, channels)[None, :]
    )
    local, through, state = local_scan((receive, key, value, log_decay, rate), channels)
    states = lax.all_gather(state, "ep", axis=0, tiled=False)
    partial = read_heads(
        lax.axis_index("ep").astype(jnp.int32).reshape(1),
        states,
        local,
        through,
        receive,
        key,
        value,
        self_token_scale.reshape(1, -1),
        head_norm_scale.reshape(1, -1),
        output_weight,
        channels,
    )
    mixer_output = lax.psum_scatter(partial, "tp", scatter_dimension=0, tiled=True)

    flat_rows = arrived.reshape(-1, arrived.shape[-1])
    expert_hidden = (
        jax.nn.silu(jnp.dot(flat_rows, routed_gate_weight[0], preferred_element_type=jnp.float32))
        * jnp.dot(flat_rows, routed_up_weight[0], preferred_element_type=jnp.float32)
    ).astype(jnp.bfloat16)
    result = jnp.dot(
        expert_hidden, routed_down_weight[0], preferred_element_type=jnp.float32
    ).astype(jnp.bfloat16)
    returned = lax.all_to_all(
        result.reshape(arrived.shape), ("ep", "tp"), split_axis=0, concat_axis=0, tiled=True
    )
    back_rows = returned.reshape(expert_count * capacity, -1)
    combine = sum(
        jnp.where(slots[j][:, None] == slot_range[None, :], route_weight[:, j : j + 1], 0.0)
        for j in range(top_count)
    )
    combine_high = lax.reduce_precision(combine, 8, 7)
    combine_low = combine - combine_high
    routed = jnp.dot(
        combine_high.astype(jnp.bfloat16), back_rows, preferred_element_type=jnp.float32
    ) + jnp.dot(combine_low.astype(jnp.bfloat16), back_rows, preferred_element_type=jnp.float32)
    shared_hidden = (
        jax.nn.silu(jnp.dot(normed_b, common_gate_weight, preferred_element_type=jnp.float32))
        * jnp.dot(normed_b, common_up_weight, preferred_element_type=jnp.float32)
    ).astype(jnp.bfloat16)
    shared_term = jnp.dot(shared_hidden, common_down_weight, preferred_element_type=jnp.float32)
    mixed_b = (routed + shared_term).astype(jnp.bfloat16)
    return (mixer_output, mixed_b)


def solution(mesh):
    in_specs = (
        P(("ep", "tp"), None),
        P(),
        P("ep", "tp"),
        P("tp"),
        P(None, "tp"),
        P(None, "tp"),
        P(None, "tp"),
        P(None, "tp"),
        P(None, "tp"),
        P("tp", None),
        P("tp"),
        P("tp", None),
        P(("ep", "tp"), None),
        P(),
        P(("ep", "tp"), None),
        P(("ep", "tp"), None),
        P(("ep", "tp"), None, None),
        P(("ep", "tp"), None, None),
        P(("ep", "tp"), None, None),
        P(),
        P(),
        P(),
    )
    out_specs = (P(("ep", "tp"), None), P(("ep", "tp"), None))
    return jax.shard_map(
        per_device, mesh=mesh, in_specs=in_specs, out_specs=out_specs, check_vma=False
    )
```

time: 491 us -> 187 us (0.38)
  other arithmetic: 203 us -> 3.61 us
  matrix products: 111 us -> 34.9 us
  starting transfers between devices: 51.1 us -> 12.3 us
  local copies, waits for them, and re-layouts: 42.3 us -> 5.12 us
  Pallas kernels: 0 us -> 29.5 us
  waiting for transfers between devices: 65.4 us -> 87.5 us
    another operation x26 -> x0, other arithmetic: 170 us -> none  [the longest x16 168 us: block_pass(): jax.scipy.linalg.solve_triangular(system, right_side, lower=True, unit_di...]
    dot_general x104 -> x11, matrix products: 97.5 us -> 30 us  [the longest x1 10.1 us: per_device(): jnp.dot(expert_hidden, routed_down_weight[0], preferred_element_type=jnp....]
    ppermute x7 -> x0, starting transfers between devices: 33.7 us -> none  [passed_along(): return lax.ppermute(value, axis, pairs)]
    all_to_all x1, waiting for transfers between devices: 44.8 us -> 15.1 us  [per_device(): lax.all_to_all(result.reshape(arrived.shape), ('ep', 'tp'), split_axis=0,...]
    pallas_call x0 -> x2, Pallas kernels: none -> 29.5 us  [the longest x1 22.5 us: local_scan(): pl.pallas_call(functools.partial(scan_kernel, channels, block_len), grid=...]
    all_gather x0 -> x1, waiting for transfers between devices: none -> 28.9 us  [per_device(): states = lax.all_gather(state, 'ep', axis=0, tiled=False)]
    all_gather x1, waiting for transfers between devices: 6.76 us -> 32.1 us  [per_device(): row_piece = lax.all_gather(normed_a, 'tp', axis=0, tiled=True)]
    mul x19 -> x0, other arithmetic: 19.4 us -> none  [the longest x8 8.03 us: block_pass(): erase_in = -unit_key * jnp.exp(cumulative - log_decay)]
  transfers between devices with their start and end apart: 11 -> 5, of which waited for: 9 -> 4; matrix products, arithmetic and copies ran while one was open for 68% -> 21% of each run, Pallas kernels for 0% -> 16%
where the time goes in v1:
time: 187 us
  waiting for transfers between devices  87.5 us (47%)
  matrix products  34.9 us (19%)
  Pallas kernels  29.5 us (16%)
  between operations  13.9 us (7%)
  starting transfers between devices  12.3 us (7%)
  local copies, waits for them, and re-layouts  5.12 us (3%)
  other arithmetic  3.61 us (2%)
    all_gather x1, waiting for transfers between devices, per_device(): row_piece = lax.all_gather(normed_a, 'tp', axis=0, tiled=True)  32.1 us
    all_gather x1, waiting for transfers between devices, per_device(): states = lax.all_gather(state, 'ep', axis=0, tiled=False)  28.9 us
    pallas_call x1, Pallas kernels, local_scan(): pl.pallas_call(functools.partial(scan_kernel, channels, block_len), grid=...  22.5 us
    all_to_all x1, waiting for transfers between devices, per_device(): lax.all_to_all(result.reshape(arrived.shape), ('ep', 'tp'), split_axis=0,...  15.1 us
    reduce_scatter x1, waiting for transfers between devices, per_device(): lax.psum_scatter(partial, 'tp', scatter_dimension=0, tiled=True)  11.3 us
    dot_general x1, matrix products, per_device(): jnp.dot(expert_hidden, routed_down_weight[0], preferred_element_type=jnp....  10.1 us
    dot_general x5, matrix products, projected(): return jnp.dot(row_piece, weight, preferred_element_type=jnp.float32)  9.87 us
    all_to_all x1, starting transfers between devices, per_device(): lax.all_to_all(outgoing, ('ep', 'tp'), split_axis=0, concat_axis=0, tiled...  7.33 us
  transfers between devices with their start and end apart: 5, of which 4 were waited for; matrix products, arithmetic and copies ran while one was open for 21% of the time, Pallas kernels for 16%

profile of v1, /device:TPU:0, one launch (start us, length us, event | category | flops | bytes accessed | tf_op | source)
XLA Modules:
  0.0 186.8 jit_solution(11726967808973958822)
XLA Ops:
  7.2 0.0 copy-start
  7.2 0.0 copy-start.5
  7.2 0.0 copy-start.1
  7.2 0.0 copy-start.4
  7.2 0.0 all-gather.4.cloned.1.call-start
  7.3 1.3 fusion.20
  8.6 2.0 %fusion.22 = bf16[128,2048]{1,0:T(8,128)(2,1)} fusion(bf16[128,2048]{1,0:T(8,128)(2,1)} %param.22, f32[2048]{0:T(1024)} %param.23, f32[128]{0:T(128)S(1)} %add_rsqrt_fusion.1), kind=kLoop, calls=%fused_computation.29 | loop fusion | flops 1048576 | bytes 1057280 | tf_op jit(solution)/shard_map/convert_element_type | solution.py:16
  10.6 0.0 all-gather.4.cloned.1.call-update
  10.7 0.0 copy-done.5
  10.7 0.2 select_reduce_fusion.1
  10.8 0.0 copy-done.1
  10.8 0.2 fusion.23
  11.1 0.0 copy-done.4
  11.1 2.1 %convolution_convert_fusion = bf16[512,2048]{1,0:T(8,128)(2,1)} fusion(s32[128]{0:T(128)S(1)} %get-tuple-element.15, s32[128]{0:T(128)S(1)} %get-tuple-element.14, bf16[128,2048]{1,0:T(8,128)(2,1)S(1)} %copy-done.1, f32[2048]{0:T(1024)S(1)} %copy-done.4, f32[128]{0:T(128)S(1)} %add_rsqrt_fusion), kind=kOutput, calls=%fused_computation.7 | convolution fusion | flops 271056896 | bytes 2631168 | tf_op jit(solution)/shard_map/dot_general | solution.py:306
  13.2 7.3 %all-to-all-start = ((bf16[32,16,2048]{2,1,0:T(8,128)(2,1)}), bf16[32,16,2048]{2,1,0:T(8,128)(2,1)S(1)}, u32[]{:S(2)}, u32[]{:S(2)}) async-start(bf16[32,16,2048]{2,1,0:T(8,128)(2,1)} %bitcast.12), calls=%async_computation.1 | async-start | bytes 4194304 | tf_op jit(solution)/shard_map/all_to_all | solution.py:308
  20.5 0.0 all-gather.6.cloned.1.call-start
  20.6 0.0 copy-done.6
  20.6 0.9 broadcast_in_dim.50
  21.4 2.1 %copy.25 = f32[512,256]{1,0:T(8,128)} copy(f32[512,256]{0,1:T(8,128)} %bitcast.69) | data formatting | bytes 1048576 | tf_op jit(solution)/shard_map/reshape | solution.py:320
  23.5 0.1 broadcast_in_dim.51
  23.6 0.1 add.85
  23.7 32.1 %all-gather.4.cloned.1.call-done = bf16[512,2048]{1,0:T(8,128)(2,1)} async-done(((bf16[128,2048]{1,0:T(8,128)(2,1)}), bf16[512,2048]{1,0:T(8,128)(2,1)}) %all-gather.4.cloned.1.call-update) | async-done | bytes 2097168 | tf_op jit(solution)/shard_map/all_gather | solution.py:311
  55.8 3.5 %fusion.77.r_ref = f32[512,256]{1,0:T(8,128)} fusion(bf16[512,2048]{1,0:T(8,128)(2,1)} %all-gather.4.cloned.1.call-done, bf16[2048,256]{1,0:T(8,128)(2,1)} %param.26), kind=kOutput, calls=%fused_computation.96 | convolution fusion | flops 536870912 | bytes 3670016 | tf_op jit(solution)/shard_map/dot_general | solution.py:315
  59.3 1.5 fusion.78.k_ref
  60.8 1.5 fusion.79.v_ref
  62.3 1.5 fusion.16.rate_ref
  63.9 0.0 copy-done.14
  63.9 1.8 fusion.31.ld_ref
  65.7 22.5 %shard_map.221 = (f32[512,256]{1,0:T(8,128)}, f32[512,256]{1,0:T(8,128)}, f32[128,256]{1,0:T(8,128)}) custom-call(f32[512,256]{1,0:T(8,128)} %fusion.77.r_ref, f32[512,256]{1,0:T(8,128)} %fusion.78.k_ref, f32[512,256]{1,0:T(8,128)} %fusion.79.v_ref, f32[512,256]{1,0:T(8,128)} %fusion.31.ld_ref, f32[512,256]{1,0:T(8,128)} %fusion.16.rate_ref), custom_call_target="tpu_custom_call" | custom-call | flops 16000000000 | bytes 4000000 | tf_op jit(solution)/shard_map/pallas_call | solution.py:166
  88.2 0.0 all-gather.6.cloned.1.call-update
  88.2 0.0 all-to-all-done
  88.2 5.9 %fusion.4 = f32[512,1024]{1,0:T(8,128)} fusion(bf16[512,2048]{1,0:T(8,128)(2,1)S(1)} %bitcast.67, bf16[1,2048,1024]{2,1,0:T(8,128)(2,1)} %param.38), kind=kOutput, calls=%fused_computation.4 | convolution fusion | flops 2147483648 | bytes 8388608 | tf_op jit(solution)/shard_map/dot_general | solution.py:344
  94.1 10.1 %fusion.6 = bf16[512,2048]{1,0:T(8,128)(2,1)} fusion(bf16[1,1024,2048]{2,1,0:T(8,128)(2,1)} %param.40, f32[512,1024]{1,0:T(8,128)} %fusion.4, bf16[512,2048]{1,0:T(8,128)(2,1)S(1)} %bitcast.68, bf16[1,2048,1024]{2,1,0:T(8,128)(2,1)} %param.39), kind=kOutput, calls=%fused_computation.6 | convolution fusion | flops 4299161600 | bytes 14680064 | tf_op jit(solution)/shard_map/dot_general | solution.py:347
  104.1 4.8 %all-to-all-start.1 = ((bf16[32,16,2048]{2,1,0:T(8,128)(2,1)}), bf16[32,16,2048]{2,1,0:T(8,128)(2,1)S(1)}, u32[]{:S(2)}, u32[]{:S(2)}) async-start(bf16[32,16,2048]{2,1,0:T(8,128)(2,1)} %bitcast.66), calls=%async_computation.2 | async-start | bytes 4194304 | tf_op jit(solution)/shard_map/all_to_all | solution.py:350
  109.0 0.0 reduce-scatter.2.cloned.1.call-start
  109.0 0.0 copy-done.8
  109.0 0.6 reshape.84.own_ref
  109.7 28.9 %all-gather.6.cloned.1.call-done = f32[1024,256]{1,0:T(8,128)} async-done(((f32[128,256]{1,0:T(8,128)}), f32[1024,256]{1,0:T(8,128)}) %all-gather.6.cloned.1.call-update) | async-done | bytes 1048592 | tf_op jit(solution)/shard_map/all_gather | solution.py:326
  138.5 7.0 %shard_map.222 = bf16[512,2048]{1,0:T(8,128)(2,1)} custom-call(s32[1]{0:T(128)} %bitcast.place_ref, f32[8,128,256]{2,1,0:T(8,128)} %bitcast.70, f32[512,256]{1,0:T(8,128)} %get-tuple-element.6.local_ref, f32[512,256]{1,0:T(8,128)} %get-tuple-element.7.through_ref, f32[512,256]{1,0:T(8,128)} %fusion.77.r_ref, f32[512,256]{1,0:T(8,128)} %fusion.78.k_ref, ...), custom_call_target="tpu_custom_call" | custom-call | flops 4000000000 | bytes 8000000 | tf_op jit(solution)/shard_map/pallas_call | solution.py:237
  145.5 0.0 reduce-scatter.2.cloned.1.call-update
  145.6 0.7 copy-done.7
  146.3 1.7 fusion.74
  148.0 3.2 %fusion.19 = f32[128,2048]{1,0:T(8,128)} fusion(bf16[256,2048]{1,0:T(8,128)(2,1)S(1)} %copy-done, bf16[2048,256]{1,0:T(8,128)(2,1)} %param.42, f32[128,256]{1,0:T(8,128)S(1)} %fusion.74, bf16[128,2048]{1,0:T(8,128)(2,1)} %param.34, f32[2048]{0:T(1024)S(1)} %copy-done.4, f32[128]{0:T(128)S(1)} %add_rsqrt_fusion), kind=kOutput, calls=%fused_computation.26 | convolution fusion | flops 269680640 | bytes 3809792 | tf_op jit(solution)/shard_map/dot_general | solution.py:367
  151.2 15.1 %all-to-all-done.1 = bf16[32,16,2048]{2,1,0:T(8,128)(2,1)S(1)} async-done(((bf16[32,16,2048]{2,1,0:T(8,128)(2,1)}), bf16[32,16,2048]{2,1,0:T(8,128)(2,1)S(1)}, u32[]{:S(2)}, u32[]{:S(2)}) %all-to-all-start.1) | async-done | bytes 2097184 | tf_op jit(solution)/shard_map/all_to_all | solution.py:350
  166.3 0.5 fusion.36
  166.9 0.7 copy-done.2
  167.5 1.4 fusion.10
  168.9 11.3 %reduce-scatter.2.cloned.1.call-done = bf16[128,2048]{1,0:T(8,128)(2,1)} async-done(((bf16[512,2048]{1,0:T(8,128)(2,1)}), bf16[128,2048]{1,0:T(8,128)(2,1)}) %reduce-scatter.2.cloned.1.call-update) | async-done | bytes 524304 | tf_op jit(solution)/shard_map/reduce_scatter | solution.py:340
  (26 shorter events, 0.1 us)
Async XLA Ops:
  7.2 140.9 %copy-start = (bf16[256,2048]{1,0:T(8,128)(2,1)S(1)}, bf16[256,2048]{1,0:T(8,128)(2,1)}, u32[]{:S(2)}) copy-start(bf16[256,2048]{1,0:T(8,128)(2,1)} %param.43) | copy-start | bytes 3145732
  7.2 3.5 %copy-start.5 = (s32[128,2]{0,1:T(2,128)S(1)}, s32[128,2]{0,1:T(2,128)}, u32[]{:S(2)}) copy-start(s32[128,2]{0,1:T(2,128)} %param.36) | copy-start | bytes 3076
  7.2 3.6 %copy-start.1 = (bf16[128,2048]{1,0:T(8,128)(2,1)S(1)}, bf16[128,2048]{1,0:T(8,128)(2,1)}, u32[]{:S(2)}) copy-start(bf16[128,2048]{1,0:T(8,128)(2,1)} %param.34) | copy-start | bytes 1572868
  7.2 3.9 %copy-start.4 = (f32[2048]{0:T(1024)S(1)}, f32[2048]{0:T(1024)}, u32[]{:S(2)}) copy-start(f32[2048]{0:T(1024)} %param.35) | copy-start | bytes 24580
  7.2 48.5 %all-gather.4.cloned.1.call-start = ((), (), s32[]{:S(2)}) async-start(), calls=%async_computation.3 | async-start | bytes 2621440 | tf_op jit(solution)/shard_map/all_gather | solution.py:311
  13.2 7.4 %copy-start.6 = (f32[512,4]{0,1:T(4,128)S(1)}, f32[512,4]{0,1:T(4,128)}, u32[]{:S(2)}) copy-start(f32[512,4]{0,1:T(4,128)} %param.24) | copy-start | bytes 24580
  13.2 10.3 %copy-start.9 = (f32[4]{0:T(128)S(1)}, f32[4]{0:T(128)}, u32[]{:S(2)}) copy-start(f32[4]{0:T(128)} %param.25) | copy-start | bytes 52
  13.2 75.0 %all-to-all-start = ((bf16[32,16,2048]{2,1,0:T(8,128)(2,1)}), bf16[32,16,2048]{2,1,0:T(8,128)(2,1)S(1)}, u32[]{:S(2)}, u32[]{:S(2)}) async-start(bf16[32,16,2048]{2,1,0:T(8,128)(2,1)} %bitcast.12), calls=%async_computation.1 | async-start | bytes 4194304 | tf_op jit(solution)/shard_map/all_to_all | solution.py:308
  20.5 118.0 %all-gather.6.cloned.1.call-start = ((), (), s32[]{:S(2)}) async-start(), calls=%async_computation.5 | async-start | bytes 1179648 | tf_op jit(solution)/shard_map/all_gather | solution.py:326
  55.8 3.5 %copy-start.10 = (bf16[512,2048]{1,0:T(8,128)(2,1)S(1)}, bf16[512,2048]{1,0:T(8,128)(2,1)}, u32[]{:S(2)}) copy-start(bf16[512,2048]{1,0:T(8,128)(2,1)} %all-gather.4.cloned.1.call-done) | copy-start | bytes 6291460
  55.8 3.5 %copy-start.11 = (bf16[2048,256]{1,0:T(8,128)(2,1)S(1)}, bf16[2048,256]{1,0:T(8,128)(2,1)}, u32[]{:S(2)}) copy-start(bf16[2048,256]{1,0:T(8,128)(2,1)} %param.27) | copy-start | bytes 3145732
  59.3 1.5 copy-start.12
  60.8 1.5 copy-start.13
  62.3 1.5 copy-start.3
  62.3 1.5 copy-start.14
  104.1 4.9 %copy-start.8 = (f32[4,64]{1,0:T(4,128)S(1)}, f32[4,64]{1,0:T(4,128)}, u32[]{:S(2)}) copy-start(f32[4,64]{1,0:T(4,128)} %param.31) | copy-start | bytes 3076
  104.1 62.2 %all-to-all-start.1 = ((bf16[32,16,2048]{2,1,0:T(8,128)(2,1)}), bf16[32,16,2048]{2,1,0:T(8,128)(2,1)S(1)}, u32[]{:S(2)}, u32[]{:S(2)}) async-start(bf16[32,16,2048]{2,1,0:T(8,128)(2,1)} %bitcast.66), calls=%async_computation.2 | async-start | bytes 4194304 | tf_op jit(solution)/shard_map/all_to_all | solution.py:350
  109.0 71.3 %reduce-scatter.2.cloned.1.call-start = ((), (), s32[]{:S(2)}) async-start(), calls=%async_computation.4 | async-start | bytes 2621440 | tf_op jit(solution)/shard_map/reduce_scatter | solution.py:340
  145.5 0.7 copy-start.7
  166.3 1.2 copy-start.2
Sparse Core Ops, SparseCore 0:
  10.8 44.9 all-gather.3
  88.3 50.1 all-gather.5
  145.7 34.5 reduce-scatter.1

commit v2 on v1

--- a/solution.py
+++ b/solution.py
@@ -14,6 +14,24 @@
     wide_values = values.astype(jnp.float32)
     inverse = lax.rsqrt(jnp.mean(wide_values * wide_values, axis=1, keepdims=True) + 1e-06)
     return (wide_values * inverse * feature_gain).astype(jnp.bfloat16)
+
+
+def gathered(block, axis):
+    peers = lax.axis_size(axis)
+    if peers & (peers - 1):
+        return lax.all_gather(block, axis, axis=0, tiled=True)
+    place = lax.axis_index(axis)
+    held = block[None]
+    bit = peers // 2
+    while bit:
+        other = lax.ppermute(held, axis, [(i, i ^ bit) for i in range(peers)])
+        upper = (place & bit) != 0
+        low, high = jnp.where(upper, other, held), jnp.where(upper, held, other)
+        held = jnp.stack([low, high], axis=0).reshape((2 * held.shape[0],) + block.shape)
+        bit //= 2
+    bits = peers.bit_length() - 1
+    order = [sum(((i >> b) & 1) << (bits - 1 - b) for b in range(bits)) for i in range(peers)]
+    return jnp.concatenate([held[i] for i in order], axis=0)
 
 
 def halves(wide):
@@ -308,7 +326,7 @@
     arrived = lax.all_to_all(outgoing, ("ep", "tp"), split_axis=0, concat_axis=0, tiled=True)
 
     normed_a = rms_rows(mixer_input_rows, mixer_norm_scale)
-    row_piece = lax.all_gather(normed_a, "tp", axis=0, tiled=True)
+    row_piece = gathered(normed_a, "tp")
     channels = self_token_scale.shape[1]
 
     def projected(weight):

time: 187 us -> 166 us (0.89)
  waiting for transfers between devices: 87.5 us -> 65.2 us
  other arithmetic: 3.61 us -> 7.08 us
  matrix products: 34.9 us -> 32.3 us
    all_gather x1 -> x0, waiting for transfers between devices: 32.1 us -> none  [per_device(): row_piece = lax.all_gather(normed_a, 'tp', axis=0, tiled=True)]
    all_gather x1, waiting for transfers between devices: 28.9 us -> 6.17 us  [per_device(): states = lax.all_gather(state, 'ep', axis=0, tiled=False)]
    all_to_all x1, waiting for transfers between devices: 0.01 us -> 16.3 us  [per_device(): lax.all_to_all(outgoing, ('ep', 'tp'), split_axis=0, concat_axis=0, tiled...]
    all_to_all x1, waiting for transfers between devices: 15.1 us -> 30.8 us  [per_device(): lax.all_to_all(result.reshape(arrived.shape), ('ep', 'tp'), split_axis=0,...]
    ppermute x0 -> x2, waiting for transfers between devices: none -> 11.9 us  [gathered(): other = lax.ppermute(held, axis, [(i, i ^ bit) for i in range(peers)])]
    reduce_scatter x1, waiting for transfers between devices: 11.3 us -> 0.01 us  [per_device(): lax.psum_scatter(partial, 'tp', scatter_dimension=0, tiled=True)]
    ppermute x0 -> x2, starting transfers between devices: none -> 3.03 us  [gathered(): other = lax.ppermute(held, axis, [(i, i ^ bit) for i in range(peers)])]
    another operation x0 -> x3, other arithmetic: none -> 3.01 us  [gathered(): jnp.stack([low, high], axis=0).reshape((2 * held.shape[0],) + block.shape)]
  transfers between devices with their start and end apart: 5 -> 6, of which waited for: 4 -> 4; matrix products, arithmetic and copies ran while one was open for 21% -> 21% of each run, Pallas kernels for 16% -> 18%
where the time goes in v2:
time: 166 us
  waiting for transfers between devices  65.2 us (39%)
  matrix products  32.3 us (19%)
  Pallas kernels  29.5 us (18%)
  between operations  14.3 us (9%)
  starting transfers between devices  13.6 us (8%)
  other arithmetic  7.08 us (4%)
  local copies, waits for them, and re-layouts  3.64 us (2%)
    all_to_all x1, waiting for transfers between devices, per_device(): lax.all_to_all(result.reshape(arrived.shape), ('ep', 'tp'), split_axis=0,...  30.8 us
    pallas_call x1, Pallas kernels, local_scan(): pl.pallas_call(functools.partial(scan_kernel, channels, block_len), grid=...  22.5 us
    all_to_all x1, waiting for transfers between devices, per_device(): lax.all_to_all(outgoing, ('ep', 'tp'), split_axis=0, concat_axis=0, tiled...  16.3 us
    ppermute x2, waiting for transfers between devices, gathered(): other = lax.ppermute(held, axis, [(i, i ^ bit) for i in range(peers)])  11.9 us
    dot_general x1, matrix products, per_device(): jnp.dot(expert_hidden, routed_down_weight[0], preferred_element_type=jnp....  10 us
    dot_general x5, matrix products, projected(): return jnp.dot(row_piece, weight, preferred_element_type=jnp.float32)  7.94 us
    pallas_call x1, Pallas kernels, read_heads(): pl.pallas_call(functools.partial(read_kernel, channels), grid=(rows // ti...  7.05 us
    all_to_all x1, starting transfers between devices, per_device(): lax.all_to_all(outgoing, ('ep', 'tp'), split_axis=0, concat_axis=0, tiled...  6.33 us
  transfers between devices with their start and end apart: 6, of which 4 were waited for; matrix products, arithmetic and copies ran while one was open for 21% of the time, Pallas kernels for 18%

profile of v2, /device:TPU:0, one launch (start us, length us, event | category | flops | bytes accessed | tf_op | source)
XLA Modules:
  0.0 165.6 jit_solution(15490676310805763958)
XLA Ops:
  7.2 0.0 copy-start
  7.2 1.3 fusion.20
  8.5 1.2 fusion.28
  9.7 3.0 %collective-permute-start = (bf16[1,128,2048]{2,1,0:T(8,128)(2,1)S(1)}, bf16[1,128,2048]{2,1,0:T(8,128)(2,1)S(1)}, u32[]{:S(2)}, u32[]{:S(2)}) collective-permute-start(bf16[1,128,2048]{2,1,0:T(8,128)(2,1)S(1)} %fusion.28), channel_id=1, source_target_pairs={{0,2},{1,3},{2,0},{3,1},{4,6},{5,7},{6,4},{7,5},{8,10},{9,11},{10,... | collective-permute-start | bytes 1572872 | tf_op jit(solution)/shard_map/ppermute | solution.py:27
  12.8 11.9 %collective-permute-done = bf16[1,128,2048]{2,1,0:T(8,128)(2,1)S(1)} collective-permute-done((bf16[1,128,2048]{2,1,0:T(8,128)(2,1)S(1)}, bf16[1,128,2048]{2,1,0:T(8,128)(2,1)S(1)}, u32[]{:S(2)}, u32[]{:S(2)}) %collective-permute-start) | collective-permute-done | bytes 524320 | tf_op jit(solution)/shard_map/ppermute | solution.py:27
  24.7 1.4 select_bitcast_fusion.3
  26.2 1.1 maximum_bitcast_fusion
  27.2 0.0 collective-permute-start.1
  27.2 0.2 select_reduce_fusion.1
  27.4 0.0 copy-done.1
  27.4 0.2 fusion.23
  27.6 2.1 %convolution_convert_fusion = bf16[512,2048]{1,0:T(8,128)(2,1)} fusion(s32[128]{0:T(128)S(1)} %get-tuple-element.23, s32[128]{0:T(128)S(1)} %get-tuple-element.22, bf16[128,2048]{1,0:T(8,128)(2,1)S(1)} %copy-done.1, f32[2048]{0:T(1024)S(1)} %copy-done.3, f32[128]{0:T(128)S(1)} %add_rsqrt_fusion), kind=kOutput, calls=%fused_computation.7 | convolution fusion | flops 271056896 | bytes 2631168 | tf_op jit(solution)/shard_map/dot_general | solution.py:324
  29.8 6.3 %all-to-all-start = ((bf16[32,16,2048]{2,1,0:T(8,128)(2,1)}), bf16[32,16,2048]{2,1,0:T(8,128)(2,1)}, u32[]{:S(2)}, u32[]{:S(2)}) async-start(bf16[32,16,2048]{2,1,0:T(8,128)(2,1)} %bitcast.23), calls=%async_computation.1 | async-start | bytes 4194304 | tf_op jit(solution)/shard_map/all_to_all | solution.py:326
  36.1 0.0 all-gather.3.cloned.1.call-start
  36.2 0.1 broadcast_in_dim.54
  36.2 0.2 copy.25
  36.5 0.1 broadcast_in_dim.55
  36.5 0.1 add.85
  36.6 0.0 collective-permute-done.1
  36.6 1.4 select_bitcast_fusion.1
  38.0 0.2 pad_maximum_fusion
  38.2 0.2 slice_bitcast_fusion.3
  38.4 0.0 copy-start.9
  38.4 0.2 pad_maximum_fusion.1
  38.6 1.0 copy-done.9
  39.6 1.5 fusion.78.r_ref
  41.1 1.5 fusion.79.k_ref
  42.6 1.6 fusion.80.v_ref
  44.2 1.5 fusion.16.rate_ref
  45.7 1.8 %fusion.32.ld_ref = f32[512,256]{1,0:T(8,128)} fusion(f32[512,256]{1,0:T(8,128)S(1)} %copy.25, bf16[512,2048]{1,0:T(8,128)(2,1)S(1)} %pad_maximum_fusion.1, bf16[2048,256]{1,0:T(8,128)(2,1)S(1)} %copy-done.13), kind=kOutput, calls=%fused_computation.42 | convolution fusion | flops 538312704 | bytes 4194304 | tf_op jit(solution)/shard_map/dot_general | solution.py:333
  47.6 22.5 %shard_map.221 = (f32[512,256]{1,0:T(8,128)}, f32[512,256]{1,0:T(8,128)}, f32[128,256]{1,0:T(8,128)}) custom-call(f32[512,256]{1,0:T(8,128)} %fusion.78.r_ref, f32[512,256]{1,0:T(8,128)} %fusion.79.k_ref, f32[512,256]{1,0:T(8,128)} %fusion.80.v_ref, f32[512,256]{1,0:T(8,128)} %fusion.32.ld_ref, f32[512,256]{1,0:T(8,128)} %fusion.16.rate_ref), custom_call_target="tpu_custom_call" | custom-call | flops 16000000000 | bytes 4000000 | tf_op jit(solution)/shard_map/pallas_call | solution.py:184
  70.1 0.0 all-gather.3.cloned.1.call-update
  70.1 16.3 %all-to-all-done = bf16[32,16,2048]{2,1,0:T(8,128)(2,1)} async-done(((bf16[32,16,2048]{2,1,0:T(8,128)(2,1)}), bf16[32,16,2048]{2,1,0:T(8,128)(2,1)}, u32[]{:S(2)}, u32[]{:S(2)}) %all-to-all-start) | async-done | bytes 2097184 | tf_op jit(solution)/shard_map/all_to_all | solution.py:326
  86.4 5.2 %fusion.4 = f32[512,1024]{1,0:T(8,128)S(1)} fusion(bf16[512,2048]{1,0:T(8,128)(2,1)} %bitcast.24, bf16[1,2048,1024]{2,1,0:T(8,128)(2,1)} %param.38), kind=kOutput, calls=%fused_computation.4 | convolution fusion | flops 2147483648 | bytes 8388608 | tf_op jit(solution)/shard_map/dot_general | solution.py:362
  91.5 10.0 %fusion.6 = bf16[512,2048]{1,0:T(8,128)(2,1)} fusion(bf16[1,1024,2048]{2,1,0:T(8,128)(2,1)} %param.40, f32[512,1024]{1,0:T(8,128)S(1)} %fusion.4, bf16[512,2048]{1,0:T(8,128)(2,1)} %bitcast.24, bf16[1,2048,1024]{2,1,0:T(8,128)(2,1)} %param.39), kind=kOutput, calls=%fused_computation.6 | convolution fusion | flops 4299161600 | bytes 14680064 | tf_op jit(solution)/shard_map/dot_general | solution.py:365
  101.6 4.2 %all-to-all-start.1 = ((bf16[32,16,2048]{2,1,0:T(8,128)(2,1)}), bf16[32,16,2048]{2,1,0:T(8,128)(2,1)S(1)}, u32[]{:S(2)}, u32[]{:S(2)}) async-start(bf16[32,16,2048]{2,1,0:T(8,128)(2,1)} %bitcast.94), calls=%async_computation.2 | async-start | bytes 4194304 | tf_op jit(solution)/shard_map/all_to_all | solution.py:368
  105.7 0.0 reduce-scatter.2.cloned.1.call-start
  105.8 0.6 reshape.92.own_ref
  106.4 6.2 %all-gather.3.cloned.1.call-done = f32[1024,256]{1,0:T(8,128)} async-done(((f32[128,256]{1,0:T(8,128)}), f32[1024,256]{1,0:T(8,128)}) %all-gather.3.cloned.1.call-update) | async-done | bytes 1048592 | tf_op jit(solution)/shard_map/all_gather | solution.py:344
  112.6 7.0 %shard_map.222 = bf16[512,2048]{1,0:T(8,128)(2,1)} custom-call(s32[1]{0:T(128)} %bitcast.place_ref, f32[8,128,256]{2,1,0:T(8,128)} %bitcast.96, f32[512,256]{1,0:T(8,128)} %get-tuple-element.6.local_ref, f32[512,256]{1,0:T(8,128)} %get-tuple-element.7.through_ref, f32[512,256]{1,0:T(8,128)} %fusion.78.r_ref, f32[512,256]{1,0:T(8,128)} %fusion.79.k_ref, ...), custom_call_target="tpu_custom_call" | custom-call | flops 4000000000 | bytes 8000000 | tf_op jit(solution)/shard_map/pallas_call | solution.py:255
  119.7 0.0 reduce-scatter.2.cloned.1.call-update
  119.7 0.7 copy-done.6
  120.4 1.7 %fusion.75 = f32[128,256]{1,0:T(8,128)S(1)} fusion(bf16[2048,256]{1,0:T(8,128)(2,1)} %param.41, bf16[128,2048]{1,0:T(8,128)(2,1)} %param.34, f32[2048]{0:T(1024)S(1)} %copy-done.3, f32[128]{0:T(128)S(1)} %add_rsqrt_fusion), kind=kOutput, calls=%fused_computation.107 | convolution fusion | flops 135266304 | bytes 1712640 | tf_op jit(solution)/shard_map/dot_general | solution.py:382
  122.1 3.2 %fusion.19 = f32[128,2048]{1,0:T(8,128)} fusion(bf16[256,2048]{1,0:T(8,128)(2,1)S(1)} %copy-done, bf16[2048,256]{1,0:T(8,128)(2,1)} %param.42, f32[128,256]{1,0:T(8,128)S(1)} %fusion.75, bf16[128,2048]{1,0:T(8,128)(2,1)} %param.34, f32[2048]{0:T(1024)S(1)} %copy-done.3, f32[128]{0:T(128)S(1)} %add_rsqrt_fusion), kind=kOutput, calls=%fused_computation.28 | convolution fusion | flops 269680640 | bytes 3809792 | tf_op jit(solution)/shard_map/dot_general | solution.py:385
  125.3 30.8 %all-to-all-done.1 = bf16[32,16,2048]{2,1,0:T(8,128)(2,1)S(1)} async-done(((bf16[32,16,2048]{2,1,0:T(8,128)(2,1)}), bf16[32,16,2048]{2,1,0:T(8,128)(2,1)S(1)}, u32[]{:S(2)}, u32[]{:S(2)}) %all-to-all-start.1) | async-done | bytes 2097184 | tf_op jit(solution)/shard_map/all_to_all | solution.py:368
  156.1 0.5 fusion.37
  156.7 0.7 copy-done.2
  157.4 1.4 fusion.10
  (31 shorter events, 0.1 us)
Async XLA Ops:
  7.2 115.0 %copy-start = (bf16[256,2048]{1,0:T(8,128)(2,1)S(1)}, bf16[256,2048]{1,0:T(8,128)(2,1)}, u32[]{:S(2)}) copy-start(bf16[256,2048]{1,0:T(8,128)(2,1)} %param.43) | copy-start | bytes 3145732
  9.7 15.0 %collective-permute-start = (bf16[1,128,2048]{2,1,0:T(8,128)(2,1)S(1)}, bf16[1,128,2048]{2,1,0:T(8,128)(2,1)S(1)}, u32[]{:S(2)}, u32[]{:S(2)}) collective-permute-start(bf16[1,128,2048]{2,1,0:T(8,128)(2,1)S(1)} %fusion.28), channel_id=1, source_target_pairs={{0,2},{1,3},{2,0},{3,1},{4,6},{5,7},{6,4},{7,5},{8,10},{9,11},{10,... | collective-permute-start | bytes 1572872 | tf_op jit(solution)/shard_map/ppermute | solution.py:27
  12.8 14.5 %copy-start.4 = (s32[128,2]{0,1:T(2,128)S(1)}, s32[128,2]{0,1:T(2,128)}, u32[]{:S(2)}) copy-start(s32[128,2]{0,1:T(2,128)} %param.36) | copy-start | bytes 3076
  12.8 14.6 %copy-start.1 = (bf16[128,2048]{1,0:T(8,128)(2,1)S(1)}, bf16[128,2048]{1,0:T(8,128)(2,1)}, u32[]{:S(2)}) copy-start(bf16[128,2048]{1,0:T(8,128)(2,1)} %param.34) | copy-start | bytes 1572868
  12.8 14.8 %copy-start.3 = (f32[2048]{0:T(1024)S(1)}, f32[2048]{0:T(1024)}, u32[]{:S(2)}) copy-start(f32[2048]{0:T(1024)} %param.35) | copy-start | bytes 24580
  27.2 9.4 %collective-permute-start.1 = (bf16[2,128,2048]{2,1,0:T(8,128)(2,1)}, bf16[2,128,2048]{2,1,0:T(8,128)(2,1)}, u32[]{:S(2)}, u32[]{:S(2)}) collective-permute-start(bf16[2,128,2048]{2,1,0:T(8,128)(2,1)} %maximum_bitcast_fusion), channel_id=1, source_target_pairs={{0,1},{1,0},{2,3},{3,2},{4,5},{5,4},{6,7},{7,6},{8,9},{9,8},{10,11... | collective-permute-start | bytes 3145736 | tf_op jit(solution)/shard_map/ppermute | solution.py:27
  29.8 6.4 %copy-start.5 = (f32[512,4]{0,1:T(4,128)S(1)}, f32[512,4]{0,1:T(4,128)}, u32[]{:S(2)}) copy-start(f32[512,4]{0,1:T(4,128)} %param.24) | copy-start | bytes 24580
  29.8 6.7 %copy-start.8 = (f32[4]{0:T(128)S(1)}, f32[4]{0:T(128)}, u32[]{:S(2)}) copy-start(f32[4]{0:T(128)} %param.25) | copy-start | bytes 52
  29.8 56.6 %all-to-all-start = ((bf16[32,16,2048]{2,1,0:T(8,128)(2,1)}), bf16[32,16,2048]{2,1,0:T(8,128)(2,1)}, u32[]{:S(2)}, u32[]{:S(2)}) async-start(bf16[32,16,2048]{2,1,0:T(8,128)(2,1)} %bitcast.23), calls=%async_computation.1 | async-start | bytes 4194304 | tf_op jit(solution)/shard_map/all_to_all | solution.py:326
  36.1 76.5 %all-gather.3.cloned.1.call-start = ((), (), s32[]{:S(2)}) async-start(), calls=%async_computation.4 | async-start | bytes 1179648 | tf_op jit(solution)/shard_map/all_gather | solution.py:344
  38.4 1.2 copy-start.9
  39.6 1.5 copy-start.10
  41.1 1.5 copy-start.11
  42.6 1.6 copy-start.12
  44.2 1.5 copy-start.13
  101.6 4.2 %copy-start.7 = (f32[4,64]{1,0:T(4,128)S(1)}, f32[4,64]{1,0:T(4,128)}, u32[]{:S(2)}) copy-start(f32[4,64]{1,0:T(4,128)} %param.31) | copy-start | bytes 3076
  101.6 54.6 %all-to-all-start.1 = ((bf16[32,16,2048]{2,1,0:T(8,128)(2,1)}), bf16[32,16,2048]{2,1,0:T(8,128)(2,1)S(1)}, u32[]{:S(2)}, u32[]{:S(2)}) async-start(bf16[32,16,2048]{2,1,0:T(8,128)(2,1)} %bitcast.94), calls=%async_computation.2 | async-start | bytes 4194304 | tf_op jit(solution)/shard_map/all_to_all | solution.py:368
  105.7 53.0 %reduce-scatter.2.cloned.1.call-start = ((), (), s32[]{:S(2)}) async-start(), calls=%async_computation.3 | async-start | bytes 2621440 | tf_op jit(solution)/shard_map/reduce_scatter | solution.py:358
  119.7 0.7 copy-start.6
  156.1 1.2 copy-start.2
Sparse Core Ops, SparseCore 0:
  70.2 42.3 all-gather.2
  119.8 38.3 reduce-scatter.1
